TPU v7x, 512 devices: a whole 4x4x16 slice. The times are simulated.
512 devices in a mesh: sp: 16 (over y, x), tp: 32 (over z, core).
Axes of the slice: x: 4, y: 4, z: 16, core: 2. Of those that a mesh axis runs over, the one named last changes fastest.
Arguments:
- tokens: bfloat16 [32768, 2048], P('sp', 'tp'), may hold values from -6 to 6
- norm_gain: float32 [2048], replicated, may hold values from 0.1 to 1.9
- w_key: bfloat16 [2048, 1024], P(None, 'tp'), may hold values from -0.125 to 0.125
- w_decay: bfloat16 [2048, 1024], P(None, 'tp'), may hold values from -0.125 to 0.125
- w_value: bfloat16 [2048, 512], replicated, may hold values from -0.125 to 0.125
- decay_bias: float32 [1024], P('tp'), may hold values from 0 to 8.5
- gate_drift: float32 [32768], P('sp'), may hold values from -1 to 1
- queries: bfloat16 [1024], P('tp'), may hold values from -6 to 6
- out_gain: float32 [4, 512], P(None, 'sp'), may hold values from 0.1 to 1.9
Outputs:
- state_cache: bfloat16 [1024, 512], P('tp', 'sp')
- first_read: float32 [4, 512], P(None, 'sp')
All inputs are finite; a program needn't handle non-finite values.
Results may differ from a plain program's by a relative error of at most 0.009.
Values may be sent and summed in bfloat16 or wider, within the bound.
A program may use at most 128 MiB of HBM per device.

v0:
```python
import jax
import jax.numpy as jnp
from jax import lax
from jax.sharding import PartitionSpec as P

QUERY_KEY_HEADS = 4
KEY_CHANNELS = 256
VALUE_CHANNELS = 512
EPS = 1e-06
GATE_NORM = 16.0


def copy_for_each(shard, axis):
    copies = jnp.broadcast_to(shard, (lax.axis_size(axis), *shard.shape))
    return lax.all_to_all(copies, axis, split_axis=0, concat_axis=0, tiled=True)


def taken_together(shard, axis):
    return copy_for_each(shard, axis).sum(axis=0)


def body(tokens, norm_gain, w_key, w_decay, w_value, decay_bias, gate_drift, queries, out_gain):
    gathered = lax.all_gather(tokens, "tp", axis=1, tiled=True)
    rows_f32 = gathered.astype(jnp.float32)
    inverse_rms = lax.rsqrt(jnp.mean(rows_f32 * rows_f32, axis=1, keepdims=True) + EPS)
    normed = (rows_f32 * inverse_rms * norm_gain[None, :]).astype(jnp.bfloat16)
    key_proj = jnp.dot(normed, w_key, preferred_element_type=jnp.float32).astype(jnp.bfloat16)
    gate_pre = jnp.dot(normed, w_decay, preferred_element_type=jnp.float32).astype(jnp.bfloat16)
    value_proj = jnp.dot(normed, w_value, preferred_element_type=jnp.float32).astype(jnp.bfloat16)
    log_decay = (
        jax.nn.log_sigmoid(gate_pre.astype(jnp.float32) + decay_bias[None, :] + gate_drift[:, None])
        / GATE_NORM
    )
    suffix = lax.cumsum(log_decay, axis=0, reverse=True)
    weighted = (key_proj.astype(jnp.float32) * jnp.exp(suffix - log_decay)).astype(jnp.bfloat16)
    partial_value = lax.dot_general(
        weighted, value_proj, (((0,), (0,)), ((), ())), preferred_element_type=jnp.float32
    )
    total_decay = suffix[0]
    channels = partial_value.shape[0]
    span_count = lax.axis_size("sp")
    spread = jnp.broadcast_to(total_decay[None, :, None], (1, channels, span_count))
    blocks, totals = (
        lax.all_to_all(partial_value[None], "sp", split_axis=2, concat_axis=0, tiled=True),
        lax.all_to_all(spread, "sp", split_axis=2, concat_axis=0, tiled=True),
    )
    later_sum = lax.cumsum(totals, axis=0, reverse=True) - totals
    matrix_state = jnp.sum(jnp.exp(later_sum) * blocks, axis=0)
    state_cache = matrix_state.astype(jnp.bfloat16)
    channel_ids = lax.axis_index("tp") * channels + jnp.arange(channels, dtype=jnp.int32)
    owners = (channel_ids // KEY_CHANNELS)[:, None] == jnp.arange(QUERY_KEY_HEADS, dtype=jnp.int32)[
        None, :
    ]
    query_of_head = jnp.where(
        owners, queries.astype(jnp.float32)[:, None] * KEY_CHANNELS ** (-0.5), 0.0
    )
    part_read = lax.dot_general(query_of_head, matrix_state, (((0,), (0,)), ((), ())))
    summed_read = taken_together(part_read, "tp")
    squares = taken_together(jnp.sum(summed_read * summed_read, axis=1), "sp")
    first_read = summed_read * lax.rsqrt(squares / VALUE_CHANNELS + EPS)[:, None] * out_gain
    return (state_cache, first_read)


def solution(mesh):
    return jax.shard_map(
        body,
        mesh=mesh,
        in_specs=(
            P("sp", "tp"),
            P(),
            P(None, "tp"),
            P(None, "tp"),
            P(),
            P("tp"),
            P("sp"),
            P("tp"),
            P(None, "sp"),
        ),
        out_specs=(P("tp", "sp"), P(None, "sp")),
        check_vma=False,
    )
```

profile of v0, /device:TPU:1, one launch (start us, length us, event | category | flops | bytes accessed | tf_op | source)
XLA Modules:
  0.0 233.4 jit_solution(4992811210441940215)
XLA Ops:
  7.2 0.0 copy-start
  7.2 0.0 copy-start.3
  7.2 0.0 all-gather.2.cloned.1.call-start
  7.2 0.7 all-gather.2.cloned.1.call-update
  7.9 0.7 convert_multiply_fusion.2
  8.6 86.0 %all-gather.2.cloned.1.call-done = bf16[2048,2048]{0,1:T(8,128)(2,1)} async-done(((bf16[2048,64]{0,1:T(8,128)(2,1)}), bf16[2048,2048]{0,1:T(8,128)(2,1)}) %all-gather.2.cloned.1.call-update) | async-done | bytes 8388624 | tf_op jit(solution)/shard_map/all_gather | solution.py:23
  94.6 5.1 %fusion = f32[2048]{0:T(1024)S(1)} fusion(bf16[2048,2048]{0,1:T(8,128)(2,1)} %all-gather.2.cloned.1.call-done), kind=kLoop, calls=%fused_computation.2 | loop fusion | flops 12580864 | bytes 8396800 | tf_op jit(solution)/shard_map/reduce_sum | solution.py:25
  99.7 0.0 copy-done.3
  99.7 0.0 copy-start.1
  99.8 0.0 copy-start.4
  99.8 0.0 copy-start.6
  99.8 8.6 %fusion.2 = bf16[2048,2048]{0,1:T(8,128)(2,1)} fusion(bf16[2048,2048]{0,1:T(8,128)(2,1)} %all-gather.2.cloned.1.call-done, f32[2048]{0:T(1024)S(1)} %copy-done.3, f32[2048]{0:T(1024)S(1)} %add_rsqrt_fusion), kind=kLoop, calls=%fused_computation.4 | loop fusion | flops 16777216 | bytes 16793600 | tf_op jit(solution)/shard_map/convert_element_type | solution.py:26
  108.4 0.0 copy-done.1
  108.4 0.0 copy-start.2
  108.4 5.0 %fusion.9 = f32[2048,32]{0,1:T(8,128)S(1)} fusion(bf16[2048,32]{0,1:T(8,128)(2,1)S(1)} %copy-done.1, bf16[2048,2048]{0,1:T(8,128)(2,1)} %fusion.2, f32[2048]{0:T(1024)S(1)} %copy-done.4, f32[32]{0:T(128)S(1)} %copy-done.6), kind=kOutput, calls=%fused_computation.14 | convolution fusion | flops 268763136 | bytes 8790144 | tf_op jit(solution)/shard_map/dot_general | solution.py:28
  113.4 0.2 fusion.13
  113.6 39.7 %reduce-window.6 = f32[32,16,128]{2,1,0:T(8,128)S(1)} reduce-window(f32[32,16,128]{2,1,0:T(8,128)S(1)} %bitcast.59, f32[]{:T(128)} %constant.32.clone.1), window={size=1x1x128 pad=0_0x0_0x0_127}, to_apply=%region_1.2 | reduce-window | flops 8323072 | bytes 524292 | tf_op jit(solution)/shard_map/reduce-window
  153.3 0.2 copy.32
  153.5 0.2 reduce-window.9
  153.7 0.1 slice.13
  153.8 0.1 broadcast_add_fusion
  153.9 0.1 copy.40
  154.0 0.0 copy-done.2
  154.0 5.0 %fusion.5 = bf16[2048,32]{0,1:T(8,128)(2,1)S(1)} fusion(bf16[2048,32]{0,1:T(8,128)(2,1)S(1)} %copy-done.2, bf16[2048,2048]{0,1:T(8,128)(2,1)} %fusion.2, f32[2048,32]{0,1:T(8,128)S(1)} %fusion.9, f32[4,8,16,128]{3,2,1,0:T(8,128)S(1)} %bitcast.56), kind=kOutput, calls=%fused_computation.9 | convolution fusion | flops 269287424 | bytes 9175040 | tf_op jit(solution)/shard_map/dot_general | solution.py:27
  159.0 0.1 slice_reduce_fusion
  159.2 0.6 broadcast_in_dim.37
  159.8 6.6 %all-to-all-start = ((f32[1,32,16]{1,0,2:T(1,128)}), f32[1,32,16]{1,0,2:T(1,128)S(1)}, u32[]{:S(2)}, u32[]{:S(2)}) async-start(f32[1,32,16]{1,0,2:T(1,128)} %broadcast_in_dim.37), calls=%async_computation | async-start | bytes 16384 | tf_op jit(solution)/shard_map/all_to_all | solution.py:45
  166.4 0.0 copy-start.5
  166.4 9.2 %fusion.10 = f32[32,512]{0,1:T(8,128)S(1)} fusion(bf16[2048,32]{0,1:T(8,128)(2,1)S(1)} %fusion.5, bf16[2048,2048]{0,1:T(8,128)(2,1)} %fusion.2, bf16[2048,512]{1,0:T(8,128)(2,1)S(1)} %copy-done), kind=kOutput, calls=%fused_computation.15 | convolution fusion | flops 4363124736 | bytes 10682368 | tf_op jit(solution)/shard_map/dot_general | solution.py:36
  175.7 0.5 broadcast.91
  176.2 1.3 reduce.3
  177.5 0.8 reshape.75
  178.3 0.0 all-to-all-done
  178.3 6.6 %all-to-all-start.1 = ((f32[16,1,1024]{2,1,0:T(1,128)}), f32[16,1,1024]{2,1,0:T(1,128)S(1)}, u32[]{:S(2)}, u32[]{:S(2)}) async-start(f32[16,1,1024]{2,1,0:T(1,128)} %reshape.75), calls=%async_computation.1 | async-start | bytes 131072 | tf_op jit(solution)/shard_map/all_to_all | solution.py:44
  185.0 6.5 %all-to-all-done.1 = f32[16,1,1024]{2,1,0:T(1,128)S(1)} async-done(((f32[16,1,1024]{2,1,0:T(1,128)}), f32[16,1,1024]{2,1,0:T(1,128)S(1)}, u32[]{:S(2)}, u32[]{:S(2)}) %all-to-all-start.1) | async-done | bytes 65568 | tf_op jit(solution)/shard_map/all_to_all | solution.py:44
  191.4 0.8 reduce.4
  192.2 0.4 reshape.76
  192.7 0.2 fusion.22
  193.0 0.1 reshape.77
  193.1 21.4 %all_to_all.44 = f32[32,1,128]{2,1,0:T(1,128)S(1)} all-to-all(f32[32,1,128]{2,1,0:T(1,128)S(1)} %reshape.77), channel_id=1, replica_groups=mesh['sp'=16,'tp'=32] {'tp'}, dimensions={0} | all-to-all | bytes 32768 | tf_op jit(solution)/shard_map/all_to_all | solution.py:15
  214.5 0.7 reduce.5
  215.2 0.1 reshape.78
  215.3 0.1 multiply_reduce_fusion.1
  215.4 0.6 broadcast_in_dim.42
  216.0 3.5 %all-to-all-start.3 = ((f32[16,1,4]{2,1,0:T(1,128)}), f32[16,1,4]{2,1,0:T(1,128)S(1)}, u32[]{:S(2)}, u32[]{:S(2)}) async-start(f32[16,1,4]{2,1,0:T(1,128)} %broadcast_in_dim.42), calls=%async_computation.3 | async-start | bytes 16384 | tf_op jit(solution)/shard_map/all_to_all | solution.py:15
  219.5 0.7 copy.31
  220.2 5.7 %all-to-all-done.3 = f32[16,1,4]{2,1,0:T(1,128)S(1)} async-done(((f32[16,1,4]{2,1,0:T(1,128)}), f32[16,1,4]{2,1,0:T(1,128)S(1)}, u32[]{:S(2)}, u32[]{:S(2)}) %all-to-all-start.3) | async-done | bytes 288 | tf_op jit(solution)/shard_map/all_to_all | solution.py:15
  225.9 0.7 multiply_multiply_fusion
  (14 shorter events, 0.3 us)
Async XLA Ops:
  7.2 159.2 %copy-start = (bf16[2048,512]{1,0:T(8,128)(2,1)S(1)}, bf16[2048,512]{1,0:T(8,128)(2,1)}, u32[]{:S(2)}) copy-start(bf16[2048,512]{1,0:T(8,128)(2,1)} %param.13) | copy-start | bytes 6291460
  7.2 92.6 %copy-start.3 = (f32[2048]{0:T(1024)S(1)}, f32[2048]{0:T(1024)}, u32[]{:S(2)}) copy-start(f32[2048]{0:T(1024)} %param.10) | copy-start | bytes 24580
  7.2 87.4 %all-gather.2.cloned.1.call-start = ((), (), s32[]{:S(2)}) async-start(), calls=%async_computation.4 | async-start | bytes 8650752 | tf_op jit(solution)/shard_map/all_gather | solution.py:23
  99.7 8.6 %copy-start.1 = (bf16[2048,32]{0,1:T(8,128)(2,1)S(1)}, bf16[2048,32]{0,1:T(8,128)(2,1)}, u32[]{:S(2)}) copy-start(bf16[2048,32]{0,1:T(8,128)(2,1)} %param.12) | copy-start | bytes 393220
  99.8 8.6 %copy-start.4 = (f32[2048]{0:T(1024)S(1)}, f32[2048]{0:T(1024)}, u32[]{:S(2)}) copy-start(f32[2048]{0:T(1024)} %param.15) | copy-start | bytes 24580
  99.8 8.6 %copy-start.6 = (f32[32]{0:T(128)S(1)}, f32[32]{0:T(128)}, u32[]{:S(2)}) copy-start(f32[32]{0:T(128)} %param.14) | copy-start | bytes 388
  108.4 45.6 %copy-start.2 = (bf16[2048,32]{0,1:T(8,128)(2,1)S(1)}, bf16[2048,32]{0,1:T(8,128)(2,1)}, u32[]{:S(2)}) copy-start(bf16[2048,32]{0,1:T(8,128)(2,1)} %param.11) | copy-start | bytes 393220
  159.8 18.5 %all-to-all-start = ((f32[1,32,16]{1,0,2:T(1,128)}), f32[1,32,16]{1,0,2:T(1,128)S(1)}, u32[]{:S(2)}, u32[]{:S(2)}) async-start(f32[1,32,16]{1,0,2:T(1,128)} %broadcast_in_dim.37), calls=%async_computation | async-start | bytes 16384 | tf_op jit(solution)/shard_map/all_to_all | solution.py:45
  166.4 59.5 %copy-start.5 = (f32[4,32]{1,0:T(4,128)S(1)}, f32[4,32]{1,0:T(4,128)}, u32[]{:S(2)}) copy-start(f32[4,32]{1,0:T(4,128)} %param.17) | copy-start | bytes 1540
  178.3 13.2 %all-to-all-start.1 = ((f32[16,1,1024]{2,1,0:T(1,128)}), f32[16,1,1024]{2,1,0:T(1,128)S(1)}, u32[]{:S(2)}, u32[]{:S(2)}) async-start(f32[16,1,1024]{2,1,0:T(1,128)} %reshape.75), calls=%async_computation.1 | async-start | bytes 131072 | tf_op jit(solution)/shard_map/all_to_all | solution.py:44
  216.0 9.9 %all-to-all-start.3 = ((f32[16,1,4]{2,1,0:T(1,128)}), f32[16,1,4]{2,1,0:T(1,128)S(1)}, u32[]{:S(2)}, u32[]{:S(2)}) async-start(f32[16,1,4]{2,1,0:T(1,128)} %broadcast_in_dim.42), calls=%async_computation.3 | async-start | bytes 16384 | tf_op jit(solution)/shard_map/all_to_all | solution.py:15
Sparse Core Ops, SparseCore 0:
  10.1 84.4 all-gather.1
where the time goes:
time: 234 us; the launch traced here: 233 us
  waiting for transfers between devices  98.8 us (42%)
  other arithmetic  58.3 us (25%)
  blocking collectives  21.4 us (9%)
  matrix products  19.5 us (8%)
  starting transfers between devices  16.8 us (7%)
  between operations  14.3 us (6%)
  local copies, waits for them, and re-layouts  4.45 us (2%)
    all_gather x1, waiting for transfers between devices, body(): gathered = lax.all_gather(tokens, 'tp', axis=1, tiled=True)  86 us
    another operation x2, other arithmetic  39.9 us
    all_to_all x1, blocking collectives, copy_for_each(): return lax.all_to_all(copies, axis, split_axis=0, concat_axis=0, tiled=True)  21.4 us
    dot_general x1, matrix products, body(): lax.dot_general(weighted, value_proj, (((0,), (0,)), ((), ())), preferred...  9.21 us
    convert_element_type x1, other arithmetic, body(): normed = (rows_f32 * inverse_rms * norm_gain[None, :]).astype(jnp.bfloat16)  8.58 us
    all_to_all x1, starting transfers between devices, body(): lax.all_to_all(partial_value[None], 'sp', split_axis=2, concat_axis=0, ti...  6.65 us
    all_to_all x1, starting transfers between devices, body(): lax.all_to_all(spread, 'sp', split_axis=2, concat_axis=0, tiled=True)  6.63 us
    all_to_all x1, waiting for transfers between devices, body(): lax.all_to_all(partial_value[None], 'sp', split_axis=2, concat_axis=0, ti...  6.47 us
  transfers between devices with their start and end apart: 4, of which 3 were waited for; matrix products, arithmetic and copies ran while one was open for 6% of the time, Pallas kernels for 0%

commit v1 on v0

--- a/solution.py
+++ b/solution.py
@@ -20,7 +20,10 @@
 
 
 def body(tokens, norm_gain, w_key, w_decay, w_value, decay_bias, gate_drift, queries, out_gain):
-    gathered = lax.all_gather(tokens, "tp", axis=1, tiled=True)
+    size = lax.axis_size("tp")
+    shards = jnp.stack([tokens for _ in range(size)])
+    shards = lax.all_to_all(shards, "tp", split_axis=0, concat_axis=0)
+    gathered = jnp.concatenate(shards, axis=1)
     rows_f32 = gathered.astype(jnp.float32)
     inverse_rms = lax.rsqrt(jnp.mean(rows_f32 * rows_f32, axis=1, keepdims=True) + EPS)
     normed = (rows_f32 * inverse_rms * norm_gain[None, :]).astype(jnp.bfloat16)

time: 234 us -> 521 us (2.23)
  waiting for transfers between devices: 98.8 us -> 373 us
  starting transfers between devices: 16.8 us -> 33.8 us
  between operations: 14.3 us -> 0.89 us
  local copies, waits for them, and re-layouts: 4.45 us -> 9.83 us
    all_to_all x0 -> x1, waiting for transfers between devices: none -> 361 us  [body(): shards = lax.all_to_all(shards, 'tp', split_axis=0, concat_axis=0)]
    all_gather x1 -> x0, waiting for transfers between devices: 86 us -> none  [body(): gathered = lax.all_gather(tokens, 'tp', axis=1, tiled=True)]
    all_to_all x0 -> x1, starting transfers between devices: none -> 16.9 us  [body(): shards = lax.all_to_all(shards, 'tp', split_axis=0, concat_axis=0)]
    another operation x2 -> x3, local copies, waits for them, and re-layouts: 0.31 us -> 5.68 us  [the longest x1 5.37 us: body(): shards = jnp.stack([tokens for _ in range(size)])]
  transfers between devices with their start and end apart: 4 -> 4, of which waited for: 3 -> 3; matrix products, arithmetic and copies ran while one was open for 6% -> 2% of each run, Pallas kernels for 0% -> 0%
where the time goes in v1:
time: 521 us
  waiting for transfers between devices  373 us (72%)
  other arithmetic  57.6 us (11%)
  starting transfers between devices  33.8 us (6%)
  blocking collectives  26.4 us (5%)
  matrix products  19.5 us (4%)
  local copies, waits for them, and re-layouts  9.83 us (2%)
    all_to_all x1, waiting for transfers between devices, body(): shards = lax.all_to_all(shards, 'tp', split_axis=0, concat_axis=0)  361 us
    another operation x2, other arithmetic  39.9 us
    all_to_all x1, blocking collectives, copy_for_each(): return lax.all_to_all(copies, axis, split_axis=0, concat_axis=0, tiled=True)  26.4 us
    all_to_all x1, starting transfers between devices, body(): shards = lax.all_to_all(shards, 'tp', split_axis=0, concat_axis=0)  16.9 us
  transfers between devices with their start and end apart: 4, of which 3 were waited for; matrix products, arithmetic and copies ran while one was open for 2% of the time, Pallas kernels for 0%

profile of v1, /device:TPU:1, one launch (start us, length us, event | category | flops | bytes accessed | tf_op | source)
XLA Modules:
  0.0 520.7 jit_solution(2359272221282271251)
XLA Ops:
  0.6 0.0 copy-start
  0.6 5.4 %stack.2 = bf16[32,2048,64]{1,2,0:T(8,128)(2,1)} broadcast(bf16[2048,64]{0,1:T(8,128)(2,1)} %param.9), dimensions={1,2} | broadcast | bytes 8650752 | tf_op jit(solution)/shard_map/stack | solution.py:24
  6.0 16.9 %all-to-all-start = ((bf16[32,2048,64]{1,2,0:T(8,128)(2,1)}), bf16[32,2048,64]{1,2,0:T(8,128)(2,1)}, u32[]{:S(2)}, u32[]{:S(2)}) async-start(bf16[32,2048,64]{1,2,0:T(8,128)(2,1)} %stack.2), calls=%async_computation | async-start | bytes 16777216 | tf_op jit(solution)/shard_map/all_to_all | solution.py:25
  22.9 0.0 copy-start.3
  23.0 0.0 copy-done.7
  23.0 360.5 %all-to-all-done = bf16[32,2048,64]{1,2,0:T(8,128)(2,1)} async-done(((bf16[32,2048,64]{1,2,0:T(8,128)(2,1)}), bf16[32,2048,64]{1,2,0:T(8,128)(2,1)}, u32[]{:S(2)}, u32[]{:S(2)}) %all-to-all-start) | async-done | bytes 8388640 | tf_op jit(solution)/shard_map/all_to_all | solution.py:25
  383.5 5.1 multiply_reduce_fusion
  388.7 0.0 copy-done.3
  388.7 0.0 copy-start.1
  388.7 0.0 copy-start.4
  388.7 0.0 copy-start.6
  388.7 8.6 %fusion.1 = bf16[2048,2048]{0,1:T(8,128)(2,1)} fusion(f32[2048]{0:T(1024)S(1)} %copy-done.3, f32[2048]{0:T(1024)S(1)} %add_rsqrt_fusion, bf16[32,2048,64]{1,2,0:T(8,128)(2,1)} %all-to-all-done), kind=kLoop, calls=%fused_computation.2 | loop fusion | flops 16777216 | bytes 16793600 | tf_op jit(solution)/shard_map/convert_element_type | solution.py:29
  397.3 0.0 copy-done.4
  397.3 0.0 copy-start.2
  397.3 5.0 fusion.8
  402.3 0.2 fusion.12
  402.5 39.7 %reduce-window.6 = f32[32,16,128]{2,1,0:T(8,128)S(1)} reduce-window(f32[32,16,128]{2,1,0:T(8,128)S(1)} %bitcast.67, f32[]{:T(128)} %constant.32.clone.1), window={size=1x1x128 pad=0_0x0_0x0_127}, to_apply=%region_1.2 | reduce-window | flops 8323072 | bytes 524292 | tf_op jit(solution)/shard_map/reduce-window
  442.2 0.2 copy.33
  442.4 0.2 reduce-window.9
  442.6 0.1 slice.13
  442.7 0.1 broadcast_add_fusion
  442.8 0.1 copy.41
  442.9 5.0 fusion.4
  448.0 0.1 slice_reduce_fusion
  448.1 0.6 broadcast_in_dim.37
  448.7 6.8 %all-to-all-start.1 = ((f32[1,32,16]{1,0,2:T(1,128)}), f32[1,32,16]{1,0,2:T(1,128)S(1)}, u32[]{:S(2)}, u32[]{:S(2)}) async-start(f32[1,32,16]{1,0,2:T(1,128)} %broadcast_in_dim.37), calls=%async_computation.1 | async-start | bytes 16384 | tf_op jit(solution)/shard_map/all_to_all | solution.py:48
  455.5 0.0 copy-start.5
  455.5 9.2 %fusion.9 = f32[32,512]{0,1:T(8,128)S(1)} fusion(bf16[2048,32]{0,1:T(8,128)(2,1)S(1)} %fusion.4, bf16[2048,2048]{0,1:T(8,128)(2,1)} %fusion.1, bf16[2048,512]{1,0:T(8,128)(2,1)S(1)} %copy-done), kind=kOutput, calls=%fused_computation.14 | convolution fusion | flops 4363124736 | bytes 10682368 | tf_op jit(solution)/shard_map/dot_general | solution.py:39
  464.7 0.5 broadcast.93
  465.2 1.3 reduce.5
  466.5 0.8 reshape.82
  467.3 0.0 all-to-all-done.1
  467.3 6.6 %all-to-all-start.2 = ((f32[16,1,1024]{2,1,0:T(1,128)}), f32[16,1,1024]{2,1,0:T(1,128)S(1)}, u32[]{:S(2)}, u32[]{:S(2)}) async-start(f32[16,1,1024]{2,1,0:T(1,128)} %reshape.82), calls=%async_computation.2 | async-start | bytes 131072 | tf_op jit(solution)/shard_map/all_to_all | solution.py:47
  474.0 6.5 %all-to-all-done.2 = f32[16,1,1024]{2,1,0:T(1,128)S(1)} async-done(((f32[16,1,1024]{2,1,0:T(1,128)}), f32[16,1,1024]{2,1,0:T(1,128)S(1)}, u32[]{:S(2)}, u32[]{:S(2)}) %all-to-all-start.2) | async-done | bytes 65568 | tf_op jit(solution)/shard_map/all_to_all | solution.py:47
  480.5 0.8 reduce.6
  481.3 0.4 reshape.83
  481.8 0.2 fusion.21
  482.0 0.1 reshape.84
  482.2 26.4 %all_to_all.49 = f32[32,1,128]{2,1,0:T(1,128)S(1)} all-to-all(f32[32,1,128]{2,1,0:T(1,128)S(1)} %reshape.84), channel_id=1, replica_groups=mesh['sp'=16,'tp'=32] {'tp'}, dimensions={0} | all-to-all | bytes 32768 | tf_op jit(solution)/shard_map/all_to_all | solution.py:15
  508.6 0.7 reduce.7
  509.3 0.1 reshape.85
  509.4 0.1 multiply_reduce_fusion.2
  509.5 0.6 broadcast_in_dim.42
  510.1 3.5 all-to-all-start.4
  513.6 0.7 copy.32
  514.3 5.7 %all-to-all-done.4 = f32[16,1,4]{2,1,0:T(1,128)S(1)} async-done(((f32[16,1,4]{2,1,0:T(1,128)}), f32[16,1,4]{2,1,0:T(1,128)S(1)}, u32[]{:S(2)}, u32[]{:S(2)}) %all-to-all-start.4) | async-done | bytes 288 | tf_op jit(solution)/shard_map/all_to_all | solution.py:15
  520.0 0.0 copy-done.5
  520.0 0.7 multiply_multiply_fusion
  (16 shorter events, 0.3 us)
Async XLA Ops:
  0.6 454.8 %copy-start = (bf16[2048,512]{1,0:T(8,128)(2,1)S(1)}, bf16[2048,512]{1,0:T(8,128)(2,1)}, u32[]{:S(2)}) copy-start(bf16[2048,512]{1,0:T(8,128)(2,1)} %param.13) | copy-start | bytes 6291460
  6.0 17.0 %copy-start.7 = (bf16[32]{0:T(256)(128)(2,1)S(1)}, bf16[32]{0:T(256)(128)(2,1)}, u32[]{:S(2)}) copy-start(bf16[32]{0:T(256)(128)(2,1)} %param.16) | copy-start | bytes 196
  6.0 377.5 %all-to-all-start = ((bf16[32,2048,64]{1,2,0:T(8,128)(2,1)}), bf16[32,2048,64]{1,2,0:T(8,128)(2,1)}, u32[]{:S(2)}, u32[]{:S(2)}) async-start(bf16[32,2048,64]{1,2,0:T(8,128)(2,1)} %stack.2), calls=%async_computation | async-start | bytes 16777216 | tf_op jit(solution)/shard_map/all_to_all | solution.py:25
  22.9 365.7 %copy-start.3 = (f32[2048]{0:T(1024)S(1)}, f32[2048]{0:T(1024)}, u32[]{:S(2)}) copy-start(f32[2048]{0:T(1024)} %param.10) | copy-start | bytes 24580
  388.7 8.6 %copy-start.1 = (bf16[2048,32]{0,1:T(8,128)(2,1)S(1)}, bf16[2048,32]{0,1:T(8,128)(2,1)}, u32[]{:S(2)}) copy-start(bf16[2048,32]{0,1:T(8,128)(2,1)} %param.12) | copy-start | bytes 393220
  388.7 8.6 %copy-start.4 = (f32[2048]{0:T(1024)S(1)}, f32[2048]{0:T(1024)}, u32[]{:S(2)}) copy-start(f32[2048]{0:T(1024)} %param.15) | copy-start | bytes 24580
  388.7 8.6 %copy-start.6 = (f32[32]{0:T(128)S(1)}, f32[32]{0:T(128)}, u32[]{:S(2)}) copy-start(f32[32]{0:T(128)} %param.14) | copy-start | bytes 388
  397.3 45.6 %copy-start.2 = (bf16[2048,32]{0,1:T(8,128)(2,1)S(1)}, bf16[2048,32]{0,1:T(8,128)(2,1)}, u32[]{:S(2)}) copy-start(bf16[2048,32]{0,1:T(8,128)(2,1)} %param.11) | copy-start | bytes 393220
  448.7 18.6 %all-to-all-start.1 = ((f32[1,32,16]{1,0,2:T(1,128)}), f32[1,32,16]{1,0,2:T(1,128)S(1)}, u32[]{:S(2)}, u32[]{:S(2)}) async-start(f32[1,32,16]{1,0,2:T(1,128)} %broadcast_in_dim.37), calls=%async_computation.1 | async-start | bytes 16384 | tf_op jit(solution)/shard_map/all_to_all | solution.py:48
  455.5 64.6 %copy-start.5 = (f32[4,32]{1,0:T(4,128)S(1)}, f32[4,32]{1,0:T(4,128)}, u32[]{:S(2)}) copy-start(f32[4,32]{1,0:T(4,128)} %param.17) | copy-start | bytes 1540
  467.3 13.2 %all-to-all-start.2 = ((f32[16,1,1024]{2,1,0:T(1,128)}), f32[16,1,1024]{2,1,0:T(1,128)S(1)}, u32[]{:S(2)}, u32[]{:S(2)}) async-start(f32[16,1,1024]{2,1,0:T(1,128)} %reshape.82), calls=%async_computation.2 | async-start | bytes 131072 | tf_op jit(solution)/shard_map/all_to_all | solution.py:47
  510.1 9.9 %all-to-all-start.4 = ((f32[16,1,4]{2,1,0:T(1,128)}), f32[16,1,4]{2,1,0:T(1,128)S(1)}, u32[]{:S(2)}, u32[]{:S(2)}) async-start(f32[16,1,4]{2,1,0:T(1,128)} %broadcast_in_dim.42), calls=%async_computation.4 | async-start | bytes 16384 | tf_op jit(solution)/shard_map/all_to_all | solution.py:15
